TPU v7x, 512 devices: a whole 4x4x16 slice. The times are simulated.
512 devices in a mesh: sp: 64 (over z, y), dp: 8 (over x, core).
Axes of the slice: x: 4, y: 4, z: 16, core: 2. Of those that a mesh axis runs over, the one named last changes fastest.
Arguments:
- val_input: bfloat16 [8192, 1536], P('sp', 'dp'), may hold values from -24 to 24, as said below
- gate_input: bfloat16 [8192, 1536], P('sp', 'dp'), may hold values from -8 to 8
- cotangent: bfloat16 [8192, 4096], P('sp'), may hold values from -16 to 16
- out_weight: bfloat16 [4096, 1536], P('sp', 'dp'), may hold values from -0.09375 to 0.09375
- conv_taps: float32 [31, 1536], P(None, 'dp'), may hold values from -1 to 1
- norm_gain: float32 [1536], P('dp'), may hold values from 0.1 to 1.9
Outputs:
- grad_val: bfloat16 [8192, 1536], P('sp', 'dp')
- grad_gate: bfloat16 [8192, 1536], P('sp', 'dp')
- grad_out_weight: float32 [4096, 1536], P('sp', 'dp')
- grad_taps: float32 [31, 1536], P(None, 'dp')
- grad_gain: float32 [1536], P('dp')
Inputs may be any that keep to these rules, and one draw needn't show every extreme that they name: `val_input`: blocks of 64 channels and blocks of 32 tokens carry their own scales.
All inputs are finite; a program needn't handle non-finite values.
Results may differ from a plain program's by a relative error of at most 0.0063.
Values may be sent and summed in bfloat16 or wider, within the bound.
No kernel may reach another device: no remote copies, remote signals or barrier semaphores. Data moves between devices by JAX's collectives and lax.ppermute only.
A program may use at most 64 MiB of HBM per device.

v0:
```python
import jax
import jax.numpy as jnp
from jax import lax
from jax.sharding import Mesh
from jax.sharding import PartitionSpec as P

SP = ("sp_0", "sp_1")
norm_floor = 0.25


def whole_of(array, axes, dim):
    if not axes:
        return array
    nearer = lax.all_gather(array, axes[-1], axis=dim, tiled=True)
    return whole_of(nearer, axes[:-1], dim)


def passed_along(value, axis, steps):
    count = lax.axis_size(axis)
    first, last = (max(0, -steps), min(count, count - steps))
    return lax.ppermute(value, axis, [(source, source + steps) for source in range(first, last)])


def from_everyone(array, axis):
    copies = jnp.broadcast_to(array, (lax.axis_size(axis), *array.shape))
    return lax.all_to_all(copies, axis, split_axis=0, concat_axis=0, tiled=True)


def taken_together(array, axis):
    return from_everyone(array, axis).sum(axis=0)


def packed_total(arrays, axis):
    ravelled, at, finished = (jnp.concatenate([a.reshape(-1) for a in arrays]), 0, [])
    running = taken_together(ravelled, axis)
    for a in arrays:
        finished.append(running[at : at + a.size].reshape(a.shape))
        at += a.size
    return tuple(finished)


def own_block(blocks, axes, turns):
    lengths = [lax.axis_size(a) for a in axes]
    blocks = blocks.reshape(*lengths, *blocks.shape[1:])
    blocks = blocks.transpose(*turns, *range(len(axes), blocks.ndim))
    blocks = blocks.reshape(-1, *blocks.shape[len(axes) :])
    for k in turns:
        blocks = lax.psum_scatter(blocks, axes[k], scatter_dimension=0, tiled=True)
    return blocks[0]


def split_up(array, dim, length):
    lengths = array.shape
    blocks = array.reshape(*lengths[:dim], length, lengths[dim] // length, *lengths[dim + 1 :])
    return jnp.moveaxis(blocks, dim, 0)


def scatter_axes(array, axes, turns, dim):
    length = lax.axis_size(axes)
    return own_block(split_up(array, dim, length), axes, turns)


def by_axis(array, axes):
    for axis in axes:
        array = lax.psum(array, axis)
    return array


def per_device(val_input, gate_input, cotangent, out_weight, conv_taps, norm_gain):
    rows_here = val_input.shape[0]
    width_dp = val_input.shape[1]
    taps = conv_taps.shape[0]
    channels = width_dp * lax.axis_size("dp")
    columns = cotangent
    grad_mix = jnp.dot(columns, whole_of(out_weight, SP, 0), preferred_element_type=jnp.float32)
    sigma_gate = jax.nn.sigmoid(gate_input.astype(jnp.float32))
    mixed_in = (val_input.astype(jnp.float32) * sigma_gate).astype(jnp.bfloat16)
    earlier = passed_along(mixed_in[rows_here - (taps - 1) :], SP, 1)
    padded_in = jnp.concatenate([earlier, lax.optimization_barrier(mixed_in)], 0).astype(
        jnp.float32
    )
    conv_out = jnp.zeros((rows_here, width_dp), jnp.float32)
    for offset in range(taps):
        conv_out = conv_out + conv_taps[offset][None, :] * padded_in[offset : offset + rows_here]
    conv_rows = lax.optimization_barrier(conv_out.astype(jnp.bfloat16)).astype(jnp.float32)
    row_sums = packed_total((jnp.sum(conv_rows, 1), jnp.sum(conv_rows * conv_rows, 1)), "dp")
    row_mean = row_sums[0][:, None] / channels
    row_var = row_sums[1][:, None] / channels - row_mean * row_mean
    inv_scale = lax.rsqrt(row_var + norm_floor)
    normed = (conv_rows - row_mean) * inv_scale
    act = normed * norm_gain[None, :]
    sigma_act = jax.nn.sigmoid(act)
    swished = (act * sigma_act).astype(jnp.bfloat16)
    columns = cotangent
    grad_out_weight = scatter_axes(
        lax.dot_general(
            columns, swished, (((0,), (0,)), ((), ())), preferred_element_type=jnp.float32
        ),
        SP,
        (1, 0),
        0,
    )
    grad_act = grad_mix * sigma_act * (1.0 + act * (1.0 - sigma_act))
    gain_part = jnp.sum(grad_act * normed, 0)
    grad_norm = grad_act * norm_gain[None, :]
    norm_sums = packed_total((jnp.sum(grad_norm, 1), jnp.sum(grad_norm * normed, 1)), "dp")
    first_sum = norm_sums[0][:, None] / channels
    second_sum = norm_sums[1][:, None] / channels
    grad_conv = (inv_scale * (grad_norm - first_sum - normed * second_sum)).astype(jnp.bfloat16)
    later = passed_along(grad_conv[: taps - 1], SP, -1)
    padded_grad = jnp.concatenate([lax.optimization_barrier(grad_conv), later], 0).astype(
        jnp.float32
    )
    own_grad = padded_grad[:rows_here]
    grad_mixed = jnp.zeros((rows_here, width_dp), jnp.float32)
    tap_list = []
    for offset in range(taps):
        back = taps - 1 - offset
        grad_mixed = grad_mixed + conv_taps[offset][None, :] * padded_grad[back : back + rows_here]
        tap_list.append(jnp.sum(own_grad * padded_in[offset : offset + rows_here], 0))
    grad_taps, grad_gain = (by_axis(jnp.stack(tap_list, 0), SP), by_axis(gain_part, SP))
    grad_rows = lax.optimization_barrier(grad_mixed.astype(jnp.bfloat16)).astype(jnp.float32)
    grad_val = (grad_rows * sigma_gate).astype(jnp.bfloat16)
    grad_gate = (
        grad_rows * val_input.astype(jnp.float32) * sigma_gate * (1.0 - sigma_gate)
    ).astype(jnp.bfloat16)
    return (grad_val, grad_gate, grad_out_weight, grad_taps, grad_gain)


def solution(mesh):
    split = Mesh(mesh.devices.reshape(16, 4, mesh.shape["dp"]), ("sp_0", "sp_1", "dp"))
    in_specs = (P(SP, "dp"), P(SP, "dp"), P(SP, None), P(SP, "dp"), P(None, "dp"), P("dp"))
    out_specs = (P(SP, "dp"), P(SP, "dp"), P(SP, "dp"), P(None, "dp"), P("dp"))
    return jax.shard_map(
        per_device, mesh=split, in_specs=in_specs, out_specs=out_specs, check_vma=False
    )
```

profile of v0, /device:TPU:2, one launch (start us, length us, event | category | flops | bytes accessed | tf_op | source)
XLA Modules:
  0.0 214.0 jit_solution(13165765928091978181)
XLA Ops:
  8.0 0.0 all-gather.2.cloned.1.call-start
  8.1 14.2 %all_gather.6 = bf16[256,192]{1,0:T(8,128)(2,1)} all-gather(bf16[64,192]{1,0:T(8,128)(2,1)} %param.9), channel_id=1, replica_groups=mesh['sp_0'=16,'sp_1'=4,'dp'=8] {'sp_1'}, dimensions={0}, use_global_device_ids=true | all-gather | bytes 122880 | tf_op jit(solution)/shard_map/all_gather | solution.py:14
  22.3 0.0 all-gather.2.cloned.1.call-update
  22.3 0.0 reduce-scatter.3.cloned.1.call-start
  22.4 0.9 fusion.1
  23.2 0.1 slice.459
  23.3 2.6 %collective-permute-start = (bf16[30,192]{0,1:T(8,128)(2,1)S(1)}, bf16[30,192]{0,1:T(8,128)(2,1)S(1)}, u32[]{:S(2)}, u32[]{:S(2)}) collective-permute-start(bf16[30,192]{0,1:T(8,128)(2,1)S(1)} %slice.459), channel_id=1, source_target_pairs={{0,8},{8,16},{16,24},{24,32},{32,40},{40,48},{48,56},{56,64},{64,7... | collective-permute-start | bytes 34568 | tf_op jit(solution)/shard_map/ppermute | solution.py:21
  25.9 1.1 fusion.62
  27.0 1.0 fusion.63
  28.0 0.1 maximum_convert_fusion
  28.1 1.8 add_convert_fusion
  29.9 10.4 %all_to_all.12 = f32[8,1,256]{2,1,0:T(1,128)S(1)} all-to-all(f32[8,1,256]{2,1,0:T(1,128)S(1)} %broadcast_in_dim.4), channel_id=1, replica_groups=mesh['sp_0'=16,'sp_1'=4,'dp'=8] {'dp'}, dimensions={0} | all-to-all | bytes 16384 | tf_op jit(solution)/shard_map/all_to_all | solution.py:26
  40.4 2.3 %convolution_bitcast_fusion = f32[4096,192]{0,1:T(8,128)} fusion(bf16[128,4096]{1,0:T(8,128)(2,1)S(1)} %copy-done, bf16[128,192]{0,1:T(8,128)(2,1)S(1)} %add_convert_fusion, f32[192]{0:T(256)S(1)} %copy-done.3, f32[128]{0:T(128)S(1)} %get-tuple-element.85, f32[128]{0:T(128)S(1)} %get-tuple-element.84), kind=kOutput, calls=%fused_computation | convolution fusion | flops 201547776 | bytes 4245248 | tf_op jit(solution)/shard_map/dot_general | solution.py:96
  42.7 5.1 %copy.19 = f32[4096,192]{1,0:T(8,128)} copy(f32[4096,192]{0,1:T(8,128)} %convolution_bitcast_fusion) | data formatting | bytes 6291456 | tf_op jit(solution)/shard_map/dot_general | solution.py:96
  47.9 4.6 %copy.20 = f32[4,16,64,192]{3,2,1,0:T(8,128)} copy(f32[4,16,64,192]{3,2,0,1:T(8,128)} %bitcast.73) | data formatting | bytes 6291456 | tf_op jit(solution)/shard_map/transpose | solution.py:45
  52.5 0.0 reduce-scatter.3.cloned.1.call-update
  52.5 0.0 reduce-scatter.5.cloned.1.call-start
  52.6 45.5 %all-gather.2.cloned.1.call-done = bf16[4096,192]{1,0:T(8,128)(2,1)} async-done(((bf16[256,192]{1,0:T(8,128)(2,1)}), bf16[4096,192]{1,0:T(8,128)(2,1)}) %all-gather.2.cloned.1.call-update) | async-done | bytes 1572880 | tf_op jit(solution)/shard_map/all_gather | solution.py:14
  98.1 2.5 %fusion.24 = (f32[192]{0:T(256)S(1)}, f32[128]{0:T(128)S(1)}, f32[128]{0:T(128)S(1)}, f32[128,192]{0,1:T(8,128)S(1)}) fusion(bf16[128,192]{0,1:T(8,128)(2,1)S(1)} %add_convert_fusion, f32[128]{0:T(128)S(1)} %get-tuple-element.85, f32[128]{0:T(128)S(1)} %get-tuple-element.84, f32[192]{0:T(256)S(1)} %copy-done.3, bf16[128,4096]{1,0:T(8,128)(2,1)S(1)} %copy-done, ...), kind=kOutput, calls=%fused_computation.32 | convolution fusion | flops 201768512 | bytes 2772480 | tf_op jit(solution)/shard_map/dot_general | solution.py:75
  100.6 10.0 %reduce-scatter.3.cloned.1.call-done = f32[16,64,192]{2,1,0:T(8,128)} async-done(((f32[64,64,192]{2,1,0:T(8,128)}), f32[16,64,192]{2,1,0:T(8,128)}) %reduce-scatter.3.cloned.1.call-update) | async-done | bytes 786448 | tf_op jit(solution)/shard_map/reduce_scatter | solution.py:48
  110.7 8.5 %all_to_all.13 = f32[8,1,256]{2,1,0:T(1,128)S(1)} all-to-all(f32[8,1,256]{2,1,0:T(1,128)S(1)} %broadcast_in_dim.5), channel_id=1, replica_groups=mesh['sp_0'=16,'sp_1'=4,'dp'=8] {'dp'}, dimensions={0} | all-to-all | bytes 16384 | tf_op jit(solution)/shard_map/all_to_all | solution.py:26
  119.2 0.1 fusion.23
  119.3 1.3 collective-permute-start.1
  120.6 4.7 %collective-permute-done.1 = bf16[30,192]{0,1:T(8,128)(2,1)S(1)} collective-permute-done((bf16[30,192]{0,1:T(8,128)(2,1)S(1)}, bf16[30,192]{0,1:T(8,128)(2,1)S(1)}, u32[]{:S(2)}, u32[]{:S(2)}) %collective-permute-start.1) | collective-permute-done | bytes 11552 | tf_op jit(solution)/shard_map/ppermute | solution.py:21
  125.4 1.8 fusion.27
  127.2 0.7 multiply_reduce_fusion.18
  127.9 0.7 multiply_reduce_fusion.9
  128.5 0.9 multiply_reduce_fusion
  129.4 0.1 stack.127
  129.5 57.1 %all-reduce = (f32[31,192]{1,0:T(8,128)S(1)}, f32[192]{0:T(256)S(1)}) all-reduce(f32[31,192]{1,0:T(8,128)S(1)} %stack.127, f32[192]{0:T(256)S(1)} %get-tuple-element.36), channel_id=1, replica_groups=mesh['sp_0'=16,'sp_1'=4,'dp'=8] {'sp_0'}, use_global_device_ids=true, to_apply=%region_39.0 | all-reduce | flops 6144 | bytes 49152 | tf_op jit(solution)/shard_map/psum | solution.py:65
  186.6 19.2 %all-reduce.1 = (f32[31,192]{1,0:T(8,128)}, f32[192]{0:T(256)}) all-reduce(f32[31,192]{1,0:T(8,128)S(1)} %get-tuple-element.41, f32[192]{0:T(256)S(1)} %get-tuple-element.42), channel_id=1, replica_groups=mesh['sp_0'=16,'sp_1'=4,'dp'=8] {'sp_1'}, use_global_device_ids=true, to_apply=%region_40.0 | all-reduce | flops 6144 | bytes 49152 | tf_op jit(solution)/shard_map/psum | solution.py:65
  205.8 0.7 fusion.5
  (21 shorter events, 0.2 us)
Async XLA Ops:
  8.0 32.4 %copy-start = (bf16[128,4096]{1,0:T(8,128)(2,1)S(1)}, bf16[128,4096]{1,0:T(8,128)(2,1)}, u32[]{:S(2)}) copy-start(bf16[128,4096]{1,0:T(8,128)(2,1)} %param.8) | copy-start | bytes 3145732
  8.0 32.4 %copy-start.3 = (f32[192]{0:T(256)S(1)}, f32[192]{0:T(256)}, u32[]{:S(2)}) copy-start(f32[192]{0:T(256)} %param.11) | copy-start | bytes 2308
  8.0 90.1 %all-gather.2.cloned.1.call-start = ((), (), s32[]{:S(2)}) async-start(), calls=%async_computation.4 | async-start | bytes 2228224 | tf_op jit(solution)/shard_map/all_gather | solution.py:14
  22.3 88.4 %reduce-scatter.3.cloned.1.call-start = ((), (), s32[]{:S(2)}) async-start(), calls=%async_computation.5 | async-start | bytes 5242880 | tf_op jit(solution)/shard_map/reduce_scatter | solution.py:48
  23.3 4.6 %collective-permute-start = (bf16[30,192]{0,1:T(8,128)(2,1)S(1)}, bf16[30,192]{0,1:T(8,128)(2,1)S(1)}, u32[]{:S(2)}, u32[]{:S(2)}) collective-permute-start(bf16[30,192]{0,1:T(8,128)(2,1)S(1)} %slice.459), channel_id=1, source_target_pairs={{0,8},{8,16},{16,24},{24,32},{32,40},{40,48},{48,56},{56,64},{64,7... | collective-permute-start | bytes 34568 | tf_op jit(solution)/shard_map/ppermute | solution.py:21
  52.5 154.0 %reduce-scatter.5.cloned.1.call-start = ((), (), s32[]{:S(2)}) async-start(), calls=%async_computation.6 | async-start | bytes 1114112 | tf_op jit(solution)/shard_map/reduce_scatter | solution.py:48
  119.3 6.0 %collective-permute-start.1 = (bf16[30,192]{0,1:T(8,128)(2,1)S(1)}, bf16[30,192]{0,1:T(8,128)(2,1)S(1)}, u32[]{:S(2)}, u32[]{:S(2)}) collective-permute-start(bf16[30,192]{0,1:T(8,128)(2,1)S(1)} %bitcast.75), channel_id=1, source_target_pairs={{8,0},{16,8},{24,16},{32,24},{40,32},{48,40},{56,48},{64,56},{72,6... | collective-permute-start | bytes 34568 | tf_op jit(solution)/shard_map/ppermute | solution.py:21
  125.3 80.5 %copy-start.1 = (bf16[128,192]{0,1:T(8,128)(2,1)S(1)}, bf16[128,192]{0,1:T(8,128)(2,1)}, u32[]{:S(2)}) copy-start(bf16[128,192]{0,1:T(8,128)(2,1)} %param.6) | copy-start | bytes 147460
  125.4 80.5 %copy-start.2 = (bf16[128,192]{0,1:T(8,128)(2,1)S(1)}, bf16[128,192]{0,1:T(8,128)(2,1)}, u32[]{:S(2)}) copy-start(bf16[128,192]{0,1:T(8,128)(2,1)} %param.7) | copy-start | bytes 147460
Sparse Core Ops, SparseCore 0:
  22.4 75.6 all-gather.1
  110.8 71.1 reduce-scatter.4
Sparse Core Ops, SparseCore 1:
  52.6 58.0 reduce-scatter.2
where the time goes:
time: 215 us; the launch traced here: 214 us
  blocking collectives  109 us (51%)
  waiting for transfers between devices  60.3 us (28%)
  between operations  15.6 us (7%)
  local copies, waits for them, and re-layouts  12 us (6%)
  other arithmetic  7.74 us (4%)
  matrix products  4.84 us (2%)
  starting transfers between devices  3.98 us (2%)
    psum x2, blocking collectives, by_axis(): array = lax.psum(array, axis)  76.3 us
    all_gather x1, waiting for transfers between devices, whole_of(): nearer = lax.all_gather(array, axes[-1], axis=dim, tiled=True)  45.5 us
    all_to_all x2, blocking collectives, from_everyone(): return lax.all_to_all(copies, axis, split_axis=0, concat_axis=0, tiled=True)  18.9 us
    all_gather x1, blocking collectives, whole_of(): nearer = lax.all_gather(array, axes[-1], axis=dim, tiled=True)  14.2 us
    reduce_scatter x2, waiting for transfers between devices, own_block(): blocks = lax.psum_scatter(blocks, axes[k], scatter_dimension=0, tiled=True)  10 us
    dot_general x1, local copies, waits for them, and re-layouts, per_device(): lax.dot_general(columns, swished, (((0,), (0,)), ((), ())), preferred_ele...  5.12 us
    ppermute x2, waiting for transfers between devices, passed_along(): lax.ppermute(value, axis, [(source, source + steps) for source in range(f...  4.69 us
    transpose x1, local copies, waits for them, and re-layouts, own_block(): blocks = blocks.transpose(*turns, *range(len(axes), blocks.ndim))  4.64 us
  transfers between devices with their start and end apart: 5, of which 3 were waited for; matrix products, arithmetic and copies ran while one was open for 11% of the time, Pallas kernels for 0%

commit v1 on v0

--- a/solution.py
+++ b/solution.py
@@ -3,6 +3,7 @@
 from jax import lax
 from jax.sharding import Mesh
 from jax.sharding import PartitionSpec as P
+from jax.lax import all_gather
 
 SP = ("sp_0", "sp_1")
 norm_floor = 0.25
@@ -62,7 +63,7 @@
 
 def by_axis(array, axes):
     for axis in axes:
-        array = lax.psum(array, axis)
+        array = jnp.sum(all_gather(array, axis), 0)
     return array
 
 

time: 215 us -> 236 us (1.098)
  the two profiles are of different devices: /device:TPU:2 before, /device:TPU:6 now
where the time goes in v1:
time: 236 us; the launch traced here: 235 us
  blocking collectives  133 us (56%)
  waiting for transfers between devices  46.5 us (20%)
  between operations  16.9 us (7%)
  local copies, waits for them, and re-layouts  15.8 us (7%)
  other arithmetic  9.02 us (4%)
  starting transfers between devices  8.99 us (4%)
  matrix products  4.84 us (2%)
    unnamed x2, blocking collectives  67.2 us
    all_gather x1, waiting for transfers between devices, whole_of(): nearer = lax.all_gather(array, axes[-1], axis=dim, tiled=True)  46.2 us
    all_gather x2, blocking collectives, by_axis(): array = jnp.sum(all_gather(array, axis), 0)  41.6 us
    all_gather x1, blocking collectives, whole_of(): nearer = lax.all_gather(array, axes[-1], axis=dim, tiled=True)  14.2 us
    all_to_all x1, blocking collectives, from_everyone(): return lax.all_to_all(copies, axis, split_axis=0, concat_axis=0, tiled=True)  9.77 us
    dot_general x1, local copies, waits for them, and re-layouts, per_device(): lax.dot_general(columns, swished, (((0,), (0,)), ((), ())), preferred_ele...  5.12 us
    all_to_all x1, starting transfers between devices, from_everyone(): return lax.all_to_all(copies, axis, split_axis=0, concat_axis=0, tiled=True)  5.06 us
  transfers between devices with their start and end apart: 6, of which 2 were waited for; matrix products, arithmetic and copies ran while one was open for 13% of the time, Pallas kernels for 0%

profile of v1, /device:TPU:6, one launch (start us, length us, event | category | flops | bytes accessed | tf_op | source)
XLA Modules:
  0.0 235.0 jit_solution(5134357420061384319)
XLA Ops:
  8.1 14.2 %all_gather.30 = bf16[256,192]{1,0:T(8,128)(2,1)} all-gather(bf16[64,192]{1,0:T(8,128)(2,1)} %param.9), channel_id=1, replica_groups=mesh['sp_0'=16,'sp_1'=4,'dp'=8] {'sp_1'}, dimensions={0}, use_global_device_ids=true | all-gather | bytes 122880 | tf_op jit(solution)/shard_map/all_gather | solution.py:15
  22.4 0.9 fusion.1
  23.3 2.6 %collective-permute-start = (bf16[30,192]{0,1:T(8,128)(2,1)S(1)}, bf16[30,192]{0,1:T(8,128)(2,1)S(1)}, u32[]{:S(2)}, u32[]{:S(2)}) collective-permute-start(bf16[30,192]{0,1:T(8,128)(2,1)S(1)} %slice.459), channel_id=1, source_target_pairs={{0,8},{8,16},{16,24},{24,32},{32,40},{40,48},{48,56},{56,64},{64,7... | collective-permute-start | bytes 34568 | tf_op jit(solution)/shard_map/ppermute | solution.py:22
  25.9 1.0 fusion.62
  26.9 1.0 fusion.63
  28.0 1.8 add_convert_fusion
  29.9 9.8 %all_to_all.12 = f32[8,1,256]{2,1,0:T(1,128)S(1)} all-to-all(f32[8,1,256]{2,1,0:T(1,128)S(1)} %broadcast_in_dim.4), channel_id=1, replica_groups=mesh['sp_0'=16,'sp_1'=4,'dp'=8] {'dp'}, dimensions={0} | all-to-all | bytes 16384 | tf_op jit(solution)/shard_map/all_to_all | solution.py:27
  39.7 2.3 convolution_bitcast_fusion
  42.0 5.1 %copy.21 = f32[4096,192]{1,0:T(8,128)} copy(f32[4096,192]{0,1:T(8,128)} %convolution_bitcast_fusion) | data formatting | bytes 6291456 | tf_op jit(solution)/shard_map/dot_general | solution.py:97
  47.1 4.7 %copy.22 = f32[4,16,64,192]{3,2,1,0:T(8,128)} copy(f32[4,16,64,192]{3,2,0,1:T(8,128)} %bitcast.77) | data formatting | bytes 6291456 | tf_op jit(solution)/shard_map/transpose | solution.py:46
  51.8 46.2 %all-gather.8.cloned.1.call-done = bf16[4096,192]{1,0:T(8,128)(2,1)} async-done(((bf16[256,192]{1,0:T(8,128)(2,1)}), bf16[4096,192]{1,0:T(8,128)(2,1)}) %all-gather.8.cloned.1.call-update) | async-done | bytes 1572880 | tf_op jit(solution)/shard_map/all_gather | solution.py:15
  98.0 2.5 %fusion.24 = (f32[192]{0:T(256)S(1)}, f32[128]{0:T(128)S(1)}, f32[128]{0:T(128)S(1)}, f32[128,192]{0,1:T(8,128)S(1)}) fusion(bf16[128,192]{0,1:T(8,128)(2,1)S(1)} %add_convert_fusion, f32[128]{0:T(128)S(1)} %get-tuple-element.81, f32[128]{0:T(128)S(1)} %get-tuple-element.80, f32[192]{0:T(256)S(1)} %copy-done.3, bf16[128,4096]{1,0:T(8,128)(2,1)S(1)} %copy-done, ...), kind=kOutput, calls=%fused_computation.32 | convolution fusion | flops 201768512 | bytes 2772480 | tf_op jit(solution)/shard_map/dot_general | solution.py:76
  100.6 0.6 broadcast_in_dim.5
  101.2 5.1 %all-to-all-start.1 = ((f32[8,1,256]{2,1,0:T(1,128)}), f32[8,1,256]{2,1,0:T(1,128)S(1)}, u32[]{:S(2)}, u32[]{:S(2)}) async-start(f32[8,1,256]{2,1,0:T(1,128)} %broadcast_in_dim.5), calls=%async_computation.1 | async-start | bytes 16384 | tf_op jit(solution)/shard_map/all_to_all | solution.py:27
  106.2 1.3 dynamic-slice.1
  107.5 1.3 dynamic-slice
  110.1 0.3 dynamic-update-slice
  110.4 0.2 reduce-scatter.3.cloned.1.call-done
  110.8 1.3 collective-permute-start.1
  112.1 59.2 %all-reduce = f32[3072]{0:T(1024)S(1)} all-reduce(f32[3072]{0:T(1024)S(1)} %dynamic-update-slice), channel_id=4, replica_groups=mesh['sp_0'=16,'sp_1'=4,'dp'=8] {'sp_0'}, use_global_device_ids=true, to_apply=%add | all-reduce | flops 3072 | bytes 24576
  171.4 0.2 dynamic-update-slice.1
  171.6 8.1 %all-reduce.1 = f32[768]{0:T(1024)S(1)} all-reduce(f32[768]{0:T(1024)S(1)} %dynamic-update-slice.1), channel_id=5, replica_groups=mesh['sp_0'=16,'sp_1'=4,'dp'=8] {'sp_1'}, use_global_device_ids=true, to_apply=%add.1 | all-reduce | flops 768 | bytes 6144
  179.7 0.6 reduce_sum.419
  180.3 1.8 fusion.27
  182.2 0.7 multiply_reduce_fusion.18
  182.9 0.7 multiply_reduce_fusion.9
  183.5 0.9 multiply_reduce_fusion
  184.4 0.1 stack.127
  184.5 29.6 %all-gather.4 = f32[16,31,192]{2,1,0:T(8,128)S(1)} all-gather(f32[1,31,192]{2,1,0:T(8,128)S(1)} %bitcast.81), channel_id=2, replica_groups=mesh['sp_0'=16,'sp_1'=4,'dp'=8] {'sp_0'}, dimensions={0}, use_global_device_ids=true | all-gather | bytes 404736 | tf_op jit(solution)/shard_map/all_gather | solution.py:66
  214.2 12.0 %all-gather.5 = f32[4,31,192]{2,1,0:T(8,128)S(1)} all-gather(f32[1,31,192]{2,1,0:T(8,128)S(1)} %bitcast.80), channel_id=3, replica_groups=mesh['sp_0'=16,'sp_1'=4,'dp'=8] {'sp_1'}, dimensions={0}, use_global_device_ids=true | all-gather | bytes 119040 | tf_op jit(solution)/shard_map/all_gather | solution.py:66
  226.2 0.6 reduce_sum.416
  226.8 0.7 fusion.5
  (36 shorter events, 0.8 us)
Async XLA Ops:
  8.0 31.7 %copy-start = (bf16[128,4096]{1,0:T(8,128)(2,1)S(1)}, bf16[128,4096]{1,0:T(8,128)(2,1)}, u32[]{:S(2)}) copy-start(bf16[128,4096]{1,0:T(8,128)(2,1)} %param.8) | copy-start | bytes 3145732
  8.0 31.7 %copy-start.3 = (f32[192]{0:T(256)S(1)}, f32[192]{0:T(256)}, u32[]{:S(2)}) copy-start(f32[192]{0:T(256)} %param.11) | copy-start | bytes 2308
  8.0 90.0 %all-gather.8.cloned.1.call-start = ((), (), s32[]{:S(2)}) async-start(), calls=%async_computation.4 | async-start | bytes 2228224 | tf_op jit(solution)/shard_map/all_gather | solution.py:15
  22.3 88.3 %reduce-scatter.3.cloned.1.call-start = ((), (), s32[]{:S(2)}) async-start(), calls=%async_computation.5 | async-start | bytes 5242880 | tf_op jit(solution)/shard_map/reduce_scatter | solution.py:49
  23.3 4.6 %collective-permute-start = (bf16[30,192]{0,1:T(8,128)(2,1)S(1)}, bf16[30,192]{0,1:T(8,128)(2,1)S(1)}, u32[]{:S(2)}, u32[]{:S(2)}) collective-permute-start(bf16[30,192]{0,1:T(8,128)(2,1)S(1)} %slice.459), channel_id=1, source_target_pairs={{0,8},{8,16},{16,24},{24,32},{32,40},{40,48},{48,56},{56,64},{64,7... | collective-permute-start | bytes 34568 | tf_op jit(solution)/shard_map/ppermute | solution.py:22
  101.2 9.2 %all-to-all-start.1 = ((f32[8,1,256]{2,1,0:T(1,128)}), f32[8,1,256]{2,1,0:T(1,128)S(1)}, u32[]{:S(2)}, u32[]{:S(2)}) async-start(f32[8,1,256]{2,1,0:T(1,128)} %broadcast_in_dim.5), calls=%async_computation.1 | async-start | bytes 16384 | tf_op jit(solution)/shard_map/all_to_all | solution.py:27
  106.2 121.3 %reduce-scatter.5.cloned.1.call-start = ((), (), s32[]{:S(2)}) async-start(), calls=%async_computation.6 | async-start | bytes 1114112 | tf_op jit(solution)/shard_map/reduce_scatter | solution.py:49
  110.8 69.5 %collective-permute-start.1 = (bf16[30,192]{0,1:T(8,128)(2,1)S(1)}, bf16[30,192]{0,1:T(8,128)(2,1)S(1)}, u32[]{:S(2)}, u32[]{:S(2)}) collective-permute-start(bf16[30,192]{0,1:T(8,128)(2,1)S(1)} %bitcast.79), channel_id=1, source_target_pairs={{8,0},{16,8},{24,16},{32,24},{40,32},{48,40},{56,48},{64,56},{72,6... | collective-permute-start | bytes 34568 | tf_op jit(solution)/shard_map/ppermute | solution.py:22
  182.2 44.7 %copy-start.1 = (bf16[128,192]{0,1:T(8,128)(2,1)S(1)}, bf16[128,192]{0,1:T(8,128)(2,1)}, u32[]{:S(2)}) copy-start(bf16[128,192]{0,1:T(8,128)(2,1)} %param.6) | copy-start | bytes 147460
  182.2 44.7 %copy-start.2 = (bf16[128,192]{0,1:T(8,128)(2,1)S(1)}, bf16[128,192]{0,1:T(8,128)(2,1)}, u32[]{:S(2)}) copy-start(bf16[128,192]{0,1:T(8,128)(2,1)} %param.7) | copy-start | bytes 147460
Sparse Core Ops, SparseCore 0:
  22.4 75.5 all-gather.7
  110.8 71.3 reduce-scatter.4
Sparse Core Ops, SparseCore 1:
  51.9 58.7 reduce-scatter.2
